TPU v7x, 32 devices: a whole 2x2x4 slice. The times are simulated.
32 devices in a mesh: ra: 2 (over core), cb: 4 (over z), dp: 4 (over y, x).
Axes of the slice: x: 2, y: 2, z: 4, core: 2. Of those that a mesh axis runs over, the one named last changes fastest.
Arguments:
- residual_in: bfloat16 [1024, 4096], P('dp', 'cb'), may hold values from -220 to 220, as said below
- gain_in: float32 [4096], P('cb'), may hold values from 0.1 to 1.9
- shift_in: float32 [4096], P('cb'), may hold values from -3 to 3
- up_weight: bfloat16 [4096, 16384], P('cb', 'ra'), may hold values from -0.09375 to 0.09375
- down_weight: bfloat16 [16384, 4096], P('ra', 'cb'), may hold values from -0.046875 to 0.046875
- gain_out: float32 [4096], P('cb'), may hold values from 0.1 to 1.9
- shift_out: float32 [4096], P('cb'), may hold values from -3 to 3
Outputs:
- layer_out: bfloat16 [1024, 4096], P('dp', 'cb')
Inputs may be any that keep to these rules, and one draw needn't show every extreme that they name: `residual_in`: real-valued activations.
All inputs are finite; a program needn't handle non-finite values.
Results may differ from a plain program's by a relative error of at most 0.0065.
Values may be sent and summed in bfloat16 or wider, within the bound.
A program may use at most 128 MiB of HBM per device.

v0:
```python
import functools

import jax
import jax.numpy as jnp
from jax import lax
from jax.experimental import pallas as pl
from jax.experimental.pallas import tpu as pltpu
from jax.sharding import PartitionSpec as P

MESH = pl.DeviceIdType.MESH
LANES = 128
STAT_ROWS = 8
CHUNK = 256
WINDOW = 4
LAG = 3
AHEAD = 8
SPLIT = 2
LAG_STEP = 7


def kernel(
    n, n_ra, x_ref, gain_in_ref, shift_in_ref, gain_out_ref, shift_out_ref, up_hbm, down_hbm, out_ref,
    up_v, down_v, tile_v, sums, from_outer, from_partner, hidden, normed, acc, acc_in, stats_in, stats_out,
    up_sem, down_sem, sums_sent, outer_got, partner_got, hidden_sent, hidden_got,
    stat_sent, stat_got, acc_sent, acc_got,
):
    me = lax.axis_index("cb")
    ra = lax.axis_index("ra")
    chunks, depth, width = up_v.shape
    tokens = x_ref.shape[0]
    steps, rows = sums.shape[0], sums.shape[1]
    split = steps // chunks
    half = n // 2
    ahead = min(AHEAD, chunks)
    side = me // half
    level = me * (1 - side) + (n - 1 - me) * side
    inner = lax.rem(me + 1 - 2 * side + n, n)
    outer = lax.rem(me - 1 + 2 * side + n, n)
    is_mid = level == half - 1
    has_outer = level > 0

    def up_copy(c):
        columns = pl.ds(pl.multiple_of(c * width, width), width)
        return pltpu.make_async_copy(up_hbm.at[:, columns], up_v.at[c], up_sem.at[c])

    def down_copy(c):
        rows = pl.ds(pl.multiple_of(c * width, width), width)
        return pltpu.make_async_copy(down_hbm.at[rows, :], down_v.at[c], down_sem.at[c])

    barrier = pltpu.get_barrier_semaphore()
    for k in range(1, n):
        pl.semaphore_signal(barrier, inc=1, device_id={"cb": lax.rem(me + k, n)}, device_id_type=MESH)
    for k in range(1, n_ra):
        pl.semaphore_signal(barrier, inc=1, device_id={"ra": lax.rem(ra + k, n_ra)}, device_id_type=MESH)

    for c in range(ahead):
        up_copy(c).start()

    def row_stats(values):
        total = jnp.sum(values, axis=1, keepdims=True)
        centred = values - total * (1.0 / depth)
        squares = jnp.sum(centred * centred, axis=1, keepdims=True)
        lane = lax.broadcasted_iota(jnp.int32, (values.shape[0], LANES), 1)
        return jnp.where(lane == 0, total, jnp.where(lane == 1, squares, 0.0))

    def stat_copy(stats, which, k, slot):
        return pltpu.make_async_remote_copy(
            src_ref=stats.at[slot], dst_ref=stats.at[slot],
            send_sem=stat_sent.at[which, k], recv_sem=stat_got.at[which, slot],
            device_id={"cb": lax.rem(me + k, n)}, device_id_type=MESH,
        )

    def send_stats(stats, which):
        for k in range(1, n):
            stat_copy(stats, which, k, me).start()

    def merged_stats(stats, which):
        for k in range(1, n):
            stat_copy(stats, which, k, lax.rem(me + k, n)).wait_recv()
        for k in range(1, n):
            stat_copy(stats, which, k, me).wait_send()
        total = stats[0][0:1]
        for j in range(1, n):
            total = total + stats[j][0:1]
        mean = total / (depth * n)
        squares = jnp.zeros_like(mean)
        for j in range(n):
            block = stats[j]
            gap = block[0:1] * (1.0 / depth) - mean
            squares = squares + (block[1:2] + depth * (gap * gap))
        scale = lax.rsqrt(squares / (depth * n) + 1e-05)
        row = lax.broadcasted_iota(jnp.int32, (LANES, tokens), 0)
        tile = jnp.where(row == 0, mean, jnp.where(row == 1, scale, 0.0)).T
        return tile[:, 0:1], tile[:, 1:2]

    values = x_ref[...].astype(jnp.float32)
    stats_in[me] = row_stats(values).T[:STAT_ROWS]
    acc[...] = jnp.zeros_like(acc)
    pl.semaphore_wait(barrier, n - 1 + n_ra - 1)
    send_stats(stats_in, 0)
    for c in range(ahead):
        down_copy(c).start()
    mean, scale = merged_stats(stats_in, 0)
    normed[...] = (
        (x_ref[...].astype(jnp.float32) - mean) * scale * gain_in_ref[...] + shift_in_ref[...]
    ).astype(jnp.bfloat16)

    def sum_copy(c, into, got):
        return pltpu.make_async_remote_copy(
            src_ref=sums.at[c], dst_ref=into.at[c], send_sem=sums_sent.at[c], recv_sem=got.at[c],
            device_id={"cb": inner}, device_id_type=MESH,
        )

    def hidden_copy(c):
        return pltpu.make_async_remote_copy(
            src_ref=hidden.at[c], dst_ref=hidden.at[c], send_sem=hidden_sent.at[c],
            recv_sem=hidden_got.at[c], device_id={"cb": outer}, device_id_type=MESH,
        )

    def block_of(r):
        return pl.ds(pl.multiple_of(r * rows, rows), rows)

    def acc_copy(k, r):
        return pltpu.make_async_remote_copy(
            src_ref=acc.at[block_of(r)], dst_ref=acc_in.at[k - 1, block_of(r)],
            send_sem=acc_sent.at[k - 1, r], recv_sem=acc_got.at[k - 1, r],
            device_id={"ra": lax.rem(ra + k, n_ra)}, device_id_type=MESH,
        )

    def inward(c):
        unit, r = c // split, lax.rem(c, split)

        @pl.when(r == 0)
        def _():
            up_copy(unit).wait()

            @pl.when(unit + ahead < chunks)
            def _():
                up_copy(unit + ahead).start()
                down_copy(unit + ahead).start()

        part = jnp.dot(normed[block_of(r)], up_v[unit], preferred_element_type=jnp.float32)

        @pl.when(has_outer)
        def _():
            sum_copy(c, from_outer, outer_got).wait_recv()
            sums[c] = (part + from_outer[c].astype(jnp.float32)).astype(jnp.bfloat16)

        @pl.when(level == 0)
        def _():
            sums[c] = part.astype(jnp.bfloat16)

        @pl.when(c >= WINDOW)
        def _():
            sum_copy(c - WINDOW, from_outer, outer_got).wait_send()

        @pl.when(is_mid)
        def _():
            sum_copy(c, from_partner, partner_got).start()

        @pl.when(level < half - 1)
        def _():
            sum_copy(c, from_outer, outer_got).start()

    def outward(c):
        @pl.when(is_mid)
        def _():
            sum_copy(c, from_partner, partner_got).wait_recv()
            full = sums[c].astype(jnp.float32) + from_partner[c].astype(jnp.float32)
            hidden[c] = jnp.square(jnp.maximum(full, 0.0)).astype(jnp.bfloat16)

        @pl.when(level < half - 1)
        def _():
            hidden_copy(c).wait_recv()

        @pl.when(has_outer)
        def _():
            hidden_copy(c).start()

        unit, r = c // split, lax.rem(c, split)

        @pl.when(r == 0)
        def _():
            down_copy(unit).wait()

        acc[block_of(r)] += jnp.dot(hidden[c], down_v[unit], preferred_element_type=jnp.float32)

        @pl.when(unit == chunks - 1)
        def _():
            for k in range(1, n_ra):
                acc_copy(k, r).start()

    lag = LAG + LAG_STEP * (half - 1 - level)

    @pl.loop(0, steps + lag)
    def _(step):
        @pl.when(step < steps)
        def _():
            inward(step)

        @pl.when(step >= lag)
        def _():
            outward(step - lag)

    @pl.loop(max(steps - WINDOW, 0), steps)
    def _(c):
        sum_copy(c, from_outer, outer_got).wait_send()

    @pl.when(has_outer)
    def _():
        @pl.loop(0, steps)
        def _(c):
            hidden_copy(c).wait_send()

    for r in range(split):
        block = pl.ds(r * rows, rows)
        for k in range(1, n_ra):
            acc_copy(k, r).wait()
        branch = acc[block]
        for k in range(1, n_ra):
            branch = branch + acc_in[k - 1, block]
        total = 2.0**0.25 * normed[block].astype(jnp.float32) + branch
        acc[block] = total
        tile_v[block] = row_stats(total)
    stats_out[me] = tile_v[...].T[:STAT_ROWS]
    send_stats(stats_out, 1)
    mean, scale = merged_stats(stats_out, 1)
    out_ref[...] = ((acc[...] - mean) * scale * gain_out_ref[...] + shift_out_ref[...]).astype(jnp.bfloat16)


def solution(mesh):
    n, n_ra = mesh.shape["cb"], mesh.shape["ra"]

    def per_device(residual_in, gain_in, shift_in, up_weight, down_weight, gain_out, shift_out):
        tokens, depth = residual_in.shape
        units = up_weight.shape[1]
        width = CHUNK if units % CHUNK == 0 else units
        chunks = units // width
        vmem = pl.BlockSpec(memory_space=pltpu.VMEM)
        hbm = pl.BlockSpec(memory_space=pl.ANY)
        split = SPLIT if tokens % (SPLIT * LANES // 2) == 0 else 1
        block = (chunks * split, tokens // split, width)
        return pl.pallas_call(
            functools.partial(kernel, n, n_ra),
            out_shape=jax.ShapeDtypeStruct((tokens, depth), jnp.bfloat16),
            in_specs=[vmem] * 5 + [hbm] * 2,
            out_specs=vmem,
            scratch_shapes=[
                pltpu.VMEM((chunks, depth, width), jnp.bfloat16),
                pltpu.VMEM((chunks, width, depth), jnp.bfloat16),
                pltpu.VMEM((tokens, LANES), jnp.float32),
                pltpu.VMEM(block, jnp.bfloat16),
                pltpu.VMEM(block, jnp.bfloat16),
                pltpu.VMEM(block, jnp.bfloat16),
                pltpu.VMEM(block, jnp.bfloat16),
                pltpu.VMEM((tokens, depth), jnp.bfloat16),
                pltpu.VMEM((tokens, depth), jnp.float32),
                pltpu.VMEM((n_ra - 1, tokens, depth), jnp.float32),
                pltpu.VMEM((n, STAT_ROWS, tokens), jnp.float32),
                pltpu.VMEM((n, STAT_ROWS, tokens), jnp.float32),
            ]
            + [pltpu.SemaphoreType.DMA((chunks,))] * 2
            + [pltpu.SemaphoreType.DMA((chunks * split,))] * 5
            + [pltpu.SemaphoreType.DMA((2, n))] * 2
            + [pltpu.SemaphoreType.DMA((n_ra - 1, split))] * 2,
            compiler_params=pltpu.CompilerParams(
                collective_id=0, has_side_effects=True, vmem_limit_bytes=64 * 1000 * 1024
            ),
        )(
            residual_in, gain_in.reshape(1, depth), shift_in.reshape(1, depth),
            gain_out.reshape(1, depth), shift_out.reshape(1, depth), up_weight, down_weight,
        )

    in_specs = (P("dp", "cb"), P("cb"), P("cb"), P("cb", "ra"), P("ra", "cb"), P("cb"), P("cb"))
    return jax.shard_map(
        per_device, mesh=mesh, in_specs=in_specs, out_specs=P("dp", "cb"), check_vma=False
    )
```

profile of v0, /device:TPU:0, one launch (start us, length us, event | category | flops | bytes accessed | tf_op | source)
XLA Modules:
  0.0 121.1 jit_solution(4374402515591965201)
XLA Ops:
  0.0 119.2 %shard_map.73 = bf16[256,1024]{1,0:T(8,128)(2,1)} custom-call(bf16[256,1024]{1,0:T(8,128)(2,1)} %x_ref.1, f32[1,1024]{1,0:T(1,128)} %bitcast.4, f32[1,1024]{1,0:T(1,128)} %bitcast.5, f32[1,1024]{1,0:T(1,128)} %bitcast.6, f32[1,1024]{1,0:T(1,128)} %bitcast.7, bf16[1024,8192]{1,0:T(8,128)(2,1)} %up_hbm.1, bf16[8192,1024]{1,0:T(8,128)(2,1)} %down_hbm.1), custom_call_target="tpu_custom_call" | custom-call | tf_op jit(solution)/shard_map/pallas_call | solution.py:243
  119.2 1.9 %copy.9 = bf16[256,1024]{1,0:T(8,128)(2,1)} copy(bf16[256,1024]{1,0:T(8,128)(2,1)} %shard_map.73) | data formatting | bytes 1048576
where the time goes:
time: 121 us
  Pallas kernels  119 us (98%)
  local copies, waits for them, and re-layouts  1.87 us (2%)
    pallas_call x1, Pallas kernels, per_device(): pl.pallas_call(functools.partial(kernel, n, n_ra), out_shape=jax.ShapeDty...  119 us

commit v1 on v0

v1 whole, which is shorter than its diff:
```python
import functools

import jax
import jax.numpy as jnp
from jax import lax
from jax.experimental import pallas as pl
from jax.experimental.pallas import tpu as pltpu
from jax.sharding import PartitionSpec as P

MESH = pl.DeviceIdType.MESH
LANES = 128
STAT_ROWS = 8
EXTRA = 16
ROWS = 64
CHUNK = 512
WINDOW = 4
RAW = 4
LAG = 3
AHEAD = 4
LAG_STEP = 7
TOTAL_AT = 3
NORM_AT = 8
LIMIT = 56


def kernel(
    n, n_ra, x_hbm, gain_in_hbm, shift_in_hbm, gain_out_hbm, shift_out_hbm, up_hbm, down_hbm, out_ref,
    x_v, vectors, up_v, down_v, tile_v, raw, raw_out, raw_in, sums, from_outer, from_partner, normed,
    acc, acc_in, stats_in, stats_out,
    x_sem, vector_sem, up_sem, down_sem, raw_sent, raw_got, sums_sent, outer_got, partner_got,
    hidden_sent, hidden_got, stat_sent, stat_got, acc_sent, acc_got,
):
    me = lax.axis_index("cb")
    ra = lax.axis_index("ra")
    chunks, depth, width = up_v.shape
    tokens = normed.shape[0]
    steps, rows = sums.shape[0], sums.shape[1]
    blocks = tokens // rows
    half = n // 2
    ahead = min(AHEAD, chunks)
    n_raw = raw_out.shape[0]
    side = me // half
    level = me * (1 - side) + (n - 1 - me) * side
    inner = lax.rem(me + 1 - 2 * side + n, n)
    outer = lax.rem(me - 1 + 2 * side + n, n)
    is_mid = level == half - 1
    has_outer = level > 0
    sends_raw = (level == 0) & (half > 1)
    takes_raw = level == 1
    hidden = from_outer

    def block_of(b):
        return pl.ds(pl.multiple_of(b * rows, rows), rows)

    def x_copy(b):
        return pltpu.make_async_copy(x_hbm.at[block_of(b)], x_v.at[block_of(b)], x_sem.at[b])

    def vector_copy(i):
        source = (gain_in_hbm, shift_in_hbm, gain_out_hbm, shift_out_hbm)[i]
        return pltpu.make_async_copy(source, vectors.at[i], vector_sem.at[i])

    def up_copy(c):
        columns = pl.ds(pl.multiple_of(c * width, width), width)
        return pltpu.make_async_copy(up_hbm.at[:, columns], up_v.at[c], up_sem.at[c])

    def down_copy(c):
        units = pl.ds(pl.multiple_of(c * width, width), width)
        return pltpu.make_async_copy(down_hbm.at[units, :], down_v.at[c], down_sem.at[c])

    barrier = pltpu.get_barrier_semaphore()
    for k in range(1, n):
        pl.semaphore_signal(barrier, inc=1, device_id={"cb": lax.rem(me + k, n)}, device_id_type=MESH)
    for k in range(1, n_ra):
        pl.semaphore_signal(barrier, inc=1, device_id={"ra": lax.rem(ra + k, n_ra)}, device_id_type=MESH)

    x_copy(0).start()
    vector_copy(0).start()
    vector_copy(1).start()
    for b in range(1, blocks):
        x_copy(b).start()
    for c in range(ahead):
        up_copy(c).start()
    vector_copy(2).start()
    vector_copy(3).start()

    def row_stats(values):
        total = jnp.sum(values, axis=1, keepdims=True)
        centred = values - total * (1.0 / depth)
        squares = jnp.sum(centred * centred, axis=1, keepdims=True)
        lane = lax.broadcasted_iota(jnp.int32, (values.shape[0], LANES), 1)
        tile_v[pl.ds(0, rows)] = jnp.where(lane == 0, total, jnp.where(lane == 1, squares, 0.0))
        return tile_v[...].T[:STAT_ROWS], centred

    def stat_copy(stats, which, b, k, slot):
        return pltpu.make_async_remote_copy(
            src_ref=stats.at[b, slot], dst_ref=stats.at[b, slot],
            send_sem=stat_sent.at[which, b, k], recv_sem=stat_got.at[which, b, slot],
            device_id={"cb": lax.rem(me + k, n)}, device_id_type=MESH,
        )

    def send_stats(stats, which, b):
        for k in range(1, n):
            stat_copy(stats, which, b, k, me).start()

    def merged_stats(stats, which, b):
        for k in range(1, n):
            stat_copy(stats, which, b, k, lax.rem(me + k, n)).wait_recv()
        for k in range(1, n):
            stat_copy(stats, which, b, k, me).wait_send()
        total = stats[b, 0][0:1]
        for j in range(1, n):
            total = total + stats[b, j][0:1]
        mean = total / (depth * n)
        squares = jnp.zeros_like(mean)
        for j in range(n):
            block = stats[b, j]
            gap = block[0:1] * (1.0 / depth) - mean
            squares = squares + (block[1:2] + depth * (gap * gap))
        scale = lax.rsqrt(squares / (depth * n) + 1e-05)
        shift = stats[b, outer][0:1] * (1.0 / depth) - mean
        row = lax.broadcasted_iota(jnp.int32, (LANES, LANES), 0)
        tile = jnp.where(row == 0, mean, jnp.where(row == 1, scale, jnp.where(row == 2, shift, 0.0)))
        return tile.T[:rows]

    def make_normed(b):
        tile = merged_stats(stats_in, 0, b)
        values = x_v[block_of(b)].astype(jnp.float32)
        normed[block_of(b)] = (
            (values - tile[:, 0:1]) * tile[:, 1:2] * vectors[0] + vectors[1]
        ).astype(jnp.bfloat16)
        return tile

    def raw_copy(c):
        return pltpu.make_async_remote_copy(
            src_ref=raw_out.at[c], dst_ref=raw_in.at[c], send_sem=raw_sent.at[c], recv_sem=raw_got.at[c],
            device_id={"cb": inner}, device_id_type=MESH,
        )

    def sum_copy(s, into, got):
        return pltpu.make_async_remote_copy(
            src_ref=sums.at[s], dst_ref=into.at[s], send_sem=sums_sent.at[s], recv_sem=got.at[s],
            device_id={"cb": inner}, device_id_type=MESH,
        )

    def hidden_copy(s):
        return pltpu.make_async_remote_copy(
            src_ref=hidden.at[s], dst_ref=hidden.at[s], send_sem=hidden_sent.at[s],
            recv_sem=hidden_got.at[s], device_id={"cb": outer}, device_id_type=MESH,
        )

    def acc_copy(k, b):
        return pltpu.make_async_remote_copy(
            src_ref=acc.at[block_of(b)], dst_ref=acc_in.at[k - 1, block_of(b)],
            send_sem=acc_sent.at[k - 1, b], recv_sem=acc_got.at[k - 1, b],
            device_id={"ra": lax.rem(ra + k, n_ra)}, device_id_type=MESH,
        )

    def want_up(c):
        up_copy(c).wait()

        @pl.when(c + ahead < chunks)
        def _():
            up_copy(c + ahead).start()
            down_copy(c + ahead).start()

    tile_v[...] = jnp.zeros_like(tile_v)
    x_copy(0).wait()
    stats_in[0, me], centred = row_stats(x_v[block_of(0)].astype(jnp.float32))
    vector_copy(0).wait()
    vector_copy(1).wait()

    @pl.when(sends_raw)
    def _():
        raw[pl.ds(0, rows)] = (centred * vectors[0]).astype(jnp.bfloat16)
        row = lax.broadcasted_iota(jnp.int32, (EXTRA, depth), 0)
        raw[pl.ds(rows, EXTRA)] = jnp.where(
            row == 0, vectors[0], jnp.where(row == 1, vectors[1], 0.0)
        ).astype(jnp.bfloat16)

    pl.semaphore_wait(barrier, n - 1 + n_ra - 1)
    send_stats(stats_in, 0, 0)

    @pl.when(sends_raw)
    def _():
        @pl.loop(0, n_raw)
        def _(c):
            want_up(c)
            raw_out[c] = jnp.dot(raw[...], up_v[c], preferred_element_type=jnp.float32).astype(jnp.bfloat16)
            raw_copy(c).start()

    @pl.loop(1, blocks)
    def _(b):
        x_copy(b).wait()
        stats_in[b, me] = row_stats(x_v[block_of(b)].astype(jnp.float32))[0]
        send_stats(stats_in, 0, b)

    for c in range(ahead):
        down_copy(c).start()
    acc[...] = jnp.zeros_like(acc)
    tile_v[pl.ds(0, rows)] = make_normed(0)

    @pl.when(~takes_raw)
    def _():
        tile_v[...] = jnp.zeros_like(tile_v)

    def inward(s):
        b, c = s // chunks, lax.rem(s, chunks)

        @pl.when((b == 0) & ((s >= n_raw) | ~sends_raw))
        def _():
            want_up(c)

        def part():
            return jnp.dot(normed[block_of(b)], up_v[c], preferred_element_type=jnp.float32)

        @pl.when(has_outer & ((s >= n_raw) | ~takes_raw))
        def _():
            mine = part()
            sum_copy(s, from_outer, outer_got).wait_recv()
            sums[s] = (mine + from_outer[s].astype(jnp.float32)).astype(jnp.bfloat16)

        @pl.when((s < n_raw) & takes_raw)
        def _():
            mine = part()
            raw_copy(s).wait_recv()
            block = raw_in[s].astype(jnp.float32)
            tile = tile_v[pl.ds(0, rows)]
            theirs = (block[:rows] + tile[:, 2:3] * block[rows : rows + 1]) * tile[:, 1:2]
            sums[s] = (mine + (theirs + block[rows + 1 : rows + 2])).astype(jnp.bfloat16)

        @pl.when((level == 0) & ((s >= n_raw) | ~sends_raw))
        def _():
            sums[s] = part().astype(jnp.bfloat16)

        @pl.when((s >= WINDOW) & ((s >= WINDOW + n_raw) | ~sends_raw))
        def _():
            sum_copy(s - WINDOW, from_outer, outer_got).wait_send()

        @pl.when((s >= WINDOW) & (s < WINDOW + n_raw) & sends_raw)
        def _():
            raw_copy(s - WINDOW).wait_send()

        @pl.when(is_mid)
        def _():
            sum_copy(s, from_partner, partner_got).start()

        @pl.when((level < half - 1) & ((s >= n_raw) | ~sends_raw))
        def _():
            sum_copy(s, from_outer, outer_got).start()

        @pl.when((c == chunks // 2) & (b + 1 < blocks))
        def _():
            make_normed(b + 1)

    def outward(s):
        b, c = s // chunks, lax.rem(s, chunks)

        @pl.when(is_mid)
        def _():
            sum_copy(s, from_partner, partner_got).wait_recv()
            full = sums[s].astype(jnp.float32) + from_partner[s].astype(jnp.float32)
            hidden[s] = jnp.square(jnp.maximum(full, 0.0)).astype(jnp.bfloat16)

        @pl.when(level < half - 1)
        def _():
            hidden_copy(s).wait_recv()

        @pl.when(has_outer)
        def _():
            hidden_copy(s).start()

        @pl.when(b == 0)
        def _():
            down_copy(c).wait()

        acc[block_of(b)] += jnp.dot(hidden[s], down_v[c], preferred_element_type=jnp.float32)

        @pl.when(c == chunks - 1)
        def _():
            for k in range(1, n_ra):
                acc_copy(k, b).start()

        @pl.when((b > 0) & (c == TOTAL_AT))
        def _():
            make_total(b - 1)

        @pl.when((b > 0) & (c == NORM_AT))
        def _():
            make_out(b - 1)

    def make_total(b):
        block = block_of(b)
        for k in range(1, n_ra):
            acc_copy(k, b).wait()
        branch = acc[block]
        for k in range(1, n_ra):
            branch = branch + acc_in[k - 1, block]
        total = 2.0**0.25 * normed[block].astype(jnp.float32) + branch
        acc[block] = total
        stats_out[b, me] = row_stats(total)[0]
        send_stats(stats_out, 1, b)

    def make_out(b):
        tile = merged_stats(stats_out, 1, b)
        out_ref[block_of(b)] = (
            (acc[block_of(b)] - tile[:, 0:1]) * tile[:, 1:2] * vectors[2] + vectors[3]
        ).astype(jnp.bfloat16)

    lag = LAG + LAG_STEP * (half - 1 - level)
    vector_copy(2).wait()
    vector_copy(3).wait()

    @pl.loop(0, steps + lag)
    def _(step):
        @pl.when(step < steps)
        def _():
            inward(step)

        @pl.when(step >= lag)
        def _():
            outward(step - lag)

    make_total(blocks - 1)

    @pl.loop(max(steps - WINDOW, 0), steps)
    def _(s):
        sum_copy(s, from_outer, outer_got).wait_send()

    @pl.when(has_outer)
    def _():
        @pl.loop(0, steps)
        def _(s):
            hidden_copy(s).wait_send()

    make_out(blocks - 1)


def solution(mesh):
    n, n_ra = mesh.shape["cb"], mesh.shape["ra"]

    def per_device(residual_in, gain_in, shift_in, up_weight, down_weight, gain_out, shift_out):
        tokens, depth = residual_in.shape
        units = up_weight.shape[1]
        width = CHUNK if units % CHUNK == 0 else units
        chunks = units // width
        rows = ROWS if tokens % ROWS == 0 else tokens
        blocks = tokens // rows
        n_raw = min(RAW, WINDOW, chunks)
        vmem = pl.BlockSpec(memory_space=pltpu.VMEM)
        hbm = pl.BlockSpec(memory_space=pl.ANY)
        pieces = (chunks * blocks, rows, width)
        vectors = [vector.reshape(1, depth) for vector in (gain_in, shift_in, gain_out, shift_out)]
        operands = [residual_in, *vectors, up_weight, down_weight]
        return pl.pallas_call(
            functools.partial(kernel, n, n_ra),
            out_shape=pltpu.VMEM((tokens, depth), jnp.bfloat16),
            in_specs=[hbm] * 7,
            out_specs=vmem,
            scratch_shapes=[
                pltpu.VMEM((tokens, depth), jnp.bfloat16),
                pltpu.VMEM((4, 1, depth), jnp.float32),
                pltpu.VMEM((chunks, depth, width), jnp.bfloat16),
                pltpu.VMEM((chunks, width, depth), jnp.bfloat16),
                pltpu.VMEM((LANES, LANES), jnp.float32),
                pltpu.VMEM((rows + EXTRA, depth), jnp.bfloat16),
                pltpu.VMEM((n_raw, rows + EXTRA, width), jnp.bfloat16),
                pltpu.VMEM((n_raw, rows + EXTRA, width), jnp.bfloat16),
                pltpu.VMEM(pieces, jnp.bfloat16),
                pltpu.VMEM(pieces, jnp.bfloat16),
                pltpu.VMEM(pieces, jnp.bfloat16),
                pltpu.VMEM((tokens, depth), jnp.bfloat16),
                pltpu.VMEM((tokens, depth), jnp.float32),
                pltpu.VMEM((n_ra - 1, tokens, depth), jnp.float32),
                pltpu.VMEM((blocks, n, STAT_ROWS, LANES), jnp.float32),
                pltpu.VMEM((blocks, n, STAT_ROWS, LANES), jnp.float32),
                pltpu.SemaphoreType.DMA((blocks,)),
                pltpu.SemaphoreType.DMA((4,)),
            ]
            + [pltpu.SemaphoreType.DMA((chunks,))] * 2
            + [pltpu.SemaphoreType.DMA((n_raw,))] * 2
            + [pltpu.SemaphoreType.DMA((chunks * blocks,))] * 5
            + [pltpu.SemaphoreType.DMA((2, blocks, n))] * 2
            + [pltpu.SemaphoreType.DMA((n_ra - 1, blocks))] * 2,
            compiler_params=pltpu.CompilerParams(
                collective_id=0, has_side_effects=True, vmem_limit_bytes=LIMIT * 1024 * 1024
            ),
        )(*(pltpu.with_memory_space_constraint(array, pltpu.HBM) for array in operands))

    in_specs = (P("dp", "cb"), P("cb"), P("cb"), P("cb", "ra"), P("ra", "cb"), P("cb"), P("cb"))
    return jax.shard_map(
        per_device, mesh=mesh, in_specs=in_specs, out_specs=P("dp", "cb"), check_vma=False
    )
```

time: 121 us -> 120 us (level)
  no operation moved by 1% of the time
where the time goes in v1:
time: 120 us
  Pallas kernels  119 us (99%)
    pallas_call x1, Pallas kernels, per_device(): pl.pallas_call(functools.partial(kernel, n, n_ra), out_shape=pltpu.VMEM((...  119 us

profile of v1, /device:TPU:0, one launch (start us, length us, event | category | flops | bytes accessed | tf_op | source)
XLA Modules:
  0.0 119.6 jit_solution(15374524127237819313)
XLA Ops:
  0.0 118.8 %shard_map.73 = bf16[256,1024]{1,0:T(8,128)(2,1)S(1)} custom-call(bf16[256,1024]{1,0:T(8,128)(2,1)} %x_hbm.1, f32[1,1024]{1,0:T(1,128)} %bitcast.4, f32[1,1024]{1,0:T(1,128)} %bitcast.5, f32[1,1024]{1,0:T(1,128)} %bitcast.6, f32[1,1024]{1,0:T(1,128)} %bitcast.7, bf16[1024,8192]{1,0:T(8,128)(2,1)} %up_hbm.1, bf16[8192,1024]{1,0:T(8,128)(2,1)} %down_hbm.1), custom_call_target="tpu_custom_call" | custom-call | tf_op jit(solution)/shard_map/pallas_call | solution.py:354
  118.8 0.8 copy.9

commit v2 on v1

--- a/solution.py
+++ b/solution.py
@@ -11,21 +11,19 @@
 LANES = 128
 STAT_ROWS = 8
 EXTRA = 16
-ROWS = 64
-CHUNK = 512
-WINDOW = 4
-RAW = 4
-LAG = 3
-AHEAD = 4
+ROWS = 128
+CHUNK = 256
+RAW = 3
+LAG = 2
+AHEAD = 8
 LAG_STEP = 7
-TOTAL_AT = 3
-NORM_AT = 8
+TOTAL_AT = 5
 LIMIT = 56
 
 
 def kernel(
     n, n_ra, x_hbm, gain_in_hbm, shift_in_hbm, gain_out_hbm, shift_out_hbm, up_hbm, down_hbm, out_ref,
-    x_v, vectors, up_v, down_v, tile_v, raw, raw_out, raw_in, sums, from_outer, from_partner, normed,
+    x_v, vectors, up_v, down_v, tile_v, raw, raw_out, raw_in, sums, from_outer, from_partner, normed, mine,
     acc, acc_in, stats_in, stats_out,
     x_sem, vector_sem, up_sem, down_sem, raw_sent, raw_got, sums_sent, outer_got, partner_got,
     hidden_sent, hidden_got, stat_sent, stat_got, acc_sent, acc_got,
@@ -163,6 +161,9 @@
             up_copy(c + ahead).start()
             down_copy(c + ahead).start()
 
+    def want_down(c):
+        down_copy(c).wait()
+
     tile_v[...] = jnp.zeros_like(tile_v)
     x_copy(0).wait()
     stats_in[0, me], centred = row_stats(x_v[block_of(0)].astype(jnp.float32))
@@ -203,77 +204,28 @@
     def _():
         tile_v[...] = jnp.zeros_like(tile_v)
 
-    def inward(s):
+    def first_pass(s, weight):
+        @pl.when(s < chunks)
+        def _():
+            weight(s)
+
+    def up_part(s):
         b, c = s // chunks, lax.rem(s, chunks)
-
-        @pl.when((b == 0) & ((s >= n_raw) | ~sends_raw))
-        def _():
-            want_up(c)
-
-        def part():
-            return jnp.dot(normed[block_of(b)], up_v[c], preferred_element_type=jnp.float32)
-
-        @pl.when(has_outer & ((s >= n_raw) | ~takes_raw))
-        def _():
-            mine = part()
-            sum_copy(s, from_outer, outer_got).wait_recv()
-            sums[s] = (mine + from_outer[s].astype(jnp.float32)).astype(jnp.bfloat16)
-
-        @pl.when((s < n_raw) & takes_raw)
-        def _():
-            mine = part()
-            raw_copy(s).wait_recv()
-            block = raw_in[s].astype(jnp.float32)
-            tile = tile_v[pl.ds(0, rows)]
-            theirs = (block[:rows] + tile[:, 2:3] * block[rows : rows + 1]) * tile[:, 1:2]
-            sums[s] = (mine + (theirs + block[rows + 1 : rows + 2])).astype(jnp.bfloat16)
-
-        @pl.when((level == 0) & ((s >= n_raw) | ~sends_raw))
-        def _():
-            sums[s] = part().astype(jnp.bfloat16)
-
-        @pl.when((s >= WINDOW) & ((s >= WINDOW + n_raw) | ~sends_raw))
-        def _():
-            sum_copy(s - WINDOW, from_outer, outer_got).wait_send()
-
-        @pl.when((s >= WINDOW) & (s < WINDOW + n_raw) & sends_raw)
-        def _():
-            raw_copy(s - WINDOW).wait_send()
-
-        @pl.when(is_mid)
-        def _():
-            sum_copy(s, from_partner, partner_got).start()
-
-        @pl.when((level < half - 1) & ((s >= n_raw) | ~sends_raw))
-        def _():
-            sum_copy(s, from_outer, outer_got).start()
+        return jnp.dot(normed[block_of(b)], up_v[c], preferred_element_type=jnp.float32)
+
+    def add_down(s):
+        b, c = s // chunks, lax.rem(s, chunks)
+        acc[block_of(b)] += jnp.dot(hidden[s], down_v[c], preferred_element_type=jnp.float32)
+
+    def after_up(s):
+        b, c = s // chunks, lax.rem(s, chunks)
 
         @pl.when((c == chunks // 2) & (b + 1 < blocks))
         def _():
             make_normed(b + 1)
 
-    def outward(s):
+    def after_down(s):
         b, c = s // chunks, lax.rem(s, chunks)
-
-        @pl.when(is_mid)
-        def _():
-            sum_copy(s, from_partner, partner_got).wait_recv()
-            full = sums[s].astype(jnp.float32) + from_partner[s].astype(jnp.float32)
-            hidden[s] = jnp.square(jnp.maximum(full, 0.0)).astype(jnp.bfloat16)
-
-        @pl.when(level < half - 1)
-        def _():
-            hidden_copy(s).wait_recv()
-
-        @pl.when(has_outer)
-        def _():
-            hidden_copy(s).start()
-
-        @pl.when(b == 0)
-        def _():
-            down_copy(c).wait()
-
-        acc[block_of(b)] += jnp.dot(hidden[s], down_v[c], preferred_element_type=jnp.float32)
 
         @pl.when(c == chunks - 1)
         def _():
@@ -284,9 +236,109 @@
         def _():
             make_total(b - 1)
 
-        @pl.when((b > 0) & (c == NORM_AT))
-        def _():
-            make_out(b - 1)
+    def take_outer(s):
+        sum_copy(s, from_outer, outer_got).wait_recv()
+        sums[s] = (mine[lax.rem(s, 2)] + from_outer[s].astype(jnp.float32)).astype(jnp.bfloat16)
+
+    def take_raw(s):
+        raw_copy(s).wait_recv()
+        block = raw_in[s].astype(jnp.float32)
+        tile = tile_v[pl.ds(0, rows)]
+        theirs = (block[:rows] + tile[:, 2:3] * block[rows : rows + 1]) * tile[:, 1:2]
+        sums[s] = (mine[lax.rem(s, 2)] + (theirs + block[rows + 1 : rows + 2])).astype(jnp.bfloat16)
+
+    def give(s, mid):
+        if mid:
+            sum_copy(s, from_partner, partner_got).start()
+        else:
+            sum_copy(s, from_outer, outer_got).start()
+
+    def take_hidden(s, mid):
+        if mid:
+            sum_copy(s, from_partner, partner_got).wait_recv()
+            full = sums[s].astype(jnp.float32) + from_partner[s].astype(jnp.float32)
+            hidden[s] = jnp.square(jnp.maximum(full, 0.0)).astype(jnp.bfloat16)
+        else:
+            hidden_copy(s).wait_recv()
+        if half > 1:
+            hidden_copy(s).start()
+
+    def relay(mid):
+        lag = LAG if mid else LAG + LAG_STEP * (half - 1 - level)
+
+        def next_up(s):
+            mine[lax.rem(s, 2)] = up_part(s)
+
+        first_pass(0, want_up)
+        next_up(0)
+
+        @pl.loop(0, lag + 1)
+        def _(s):
+            if half > 1:
+                @pl.when((s < n_raw) & takes_raw)
+                def _():
+                    take_raw(s)
+
+                @pl.when((s >= n_raw) | ~takes_raw)
+                def _():
+                    take_outer(s)
+            else:
+                sums[s] = mine[lax.rem(s, 2)].astype(jnp.bfloat16)
+            give(s, mid)
+            first_pass(s + 1, want_up)
+            next_up(s + 1)
+            after_up(s + 1)
+
+            @pl.when(s == lag)
+            def _():
+                take_hidden(s - lag, mid)
+
+        @pl.loop(lag + 1, steps - 1)
+        def _(s):
+            if half > 1:
+                take_outer(s)
+            else:
+                sums[s] = mine[lax.rem(s, 2)].astype(jnp.bfloat16)
+            give(s, mid)
+            first_pass(s + 1, want_up)
+            first_pass(s - lag - 1, want_down)
+            add_down(s - lag - 1)
+            next_up(s + 1)
+            take_hidden(s - lag, mid)
+            after_up(s + 1)
+            after_down(s - lag - 1)
+
+        if half > 1:
+            take_outer(steps - 1)
+        else:
+            sums[steps - 1] = mine[(steps - 1) % 2].astype(jnp.bfloat16)
+        give(steps - 1, mid)
+
+        @pl.loop(steps - 1, steps + lag)
+        def _(s):
+            first_pass(s - lag - 1, want_down)
+            add_down(s - lag - 1)
+            after_down(s - lag - 1)
+            take_hidden(s - lag, mid)
+
+        first_pass(steps - 1, want_down)
+        add_down(steps - 1)
+        after_down(steps - 1)
+
+    def source():
+        @pl.loop(n_raw, steps)
+        def _(s):
+            first_pass(s, want_up)
+            sums[s] = up_part(s).astype(jnp.bfloat16)
+            sum_copy(s, from_outer, outer_got).start()
+            after_up(s)
+
+        @pl.loop(0, steps)
+        def _(s):
+            hidden_copy(s).wait_recv()
+            first_pass(s, want_down)
+            add_down(s)
+            after_down(s)
 
     def make_total(b):
         block = block_of(b)
@@ -306,23 +358,23 @@
             (acc[block_of(b)] - tile[:, 0:1]) * tile[:, 1:2] * vectors[2] + vectors[3]
         ).astype(jnp.bfloat16)
 
-    lag = LAG + LAG_STEP * (half - 1 - level)
     vector_copy(2).wait()
     vector_copy(3).wait()
-
-    @pl.loop(0, steps + lag)
-    def _(step):
-        @pl.when(step < steps)
-        def _():
-            inward(step)
-
-        @pl.when(step >= lag)
-        def _():
-            outward(step - lag)
+    pl.when(is_mid)(functools.partial(relay, True))
+    if half > 1:
+        pl.when(level == 0)(source)
+    if half > 2:
+        pl.when((level > 0) & (level < half - 1))(functools.partial(relay, False))
 
     make_total(blocks - 1)
 
-    @pl.loop(max(steps - WINDOW, 0), steps)
+    @pl.when(sends_raw)
+    def _():
+        @pl.loop(0, n_raw)
+        def _(c):
+            raw_copy(c).wait_send()
+
+    @pl.loop(jnp.where(sends_raw, n_raw, 0), steps)
     def _(s):
         sum_copy(s, from_outer, outer_got).wait_send()
 
@@ -332,7 +384,9 @@
         def _(s):
             hidden_copy(s).wait_send()
 
-    make_out(blocks - 1)
+    @pl.loop(0, blocks)
+    def _(b):
+        make_out(b)
 
 
 def solution(mesh):
@@ -345,7 +399,7 @@
         chunks = units // width
         rows = ROWS if tokens % ROWS == 0 else tokens
         blocks = tokens // rows
-        n_raw = min(RAW, WINDOW, chunks)
+        n_raw = min(RAW, LAG + 1, chunks)
         vmem = pl.BlockSpec(memory_space=pltpu.VMEM)
         hbm = pl.BlockSpec(memory_space=pl.ANY)
         pieces = (chunks * blocks, rows, width)
@@ -369,6 +423,7 @@
                 pltpu.VMEM(pieces, jnp.bfloat16),
                 pltpu.VMEM(pieces, jnp.bfloat16),
                 pltpu.VMEM((tokens, depth), jnp.bfloat16),
+                pltpu.VMEM((2, rows, width), jnp.float32),
                 pltpu.VMEM((tokens, depth), jnp.float32),
                 pltpu.VMEM((n_ra - 1, tokens, depth), jnp.float32),
                 pltpu.VMEM((blocks, n, STAT_ROWS, LANES), jnp.float32),

time: 120 us -> 116 us (0.967)
  Pallas kernels: 119 us -> 115 us
    pallas_call x1, Pallas kernels: 119 us -> 115 us  [per_device(): pl.pallas_call(functools.partial(kernel, n, n_ra), out_shape=pltpu.VMEM((...]
where the time goes in v2:
time: 116 us
  Pallas kernels  115 us (99%)
    pallas_call x1, Pallas kernels, per_device(): pl.pallas_call(functools.partial(kernel, n, n_ra), out_shape=pltpu.VMEM((...  115 us

profile of v2, /device:TPU:0, one launch (start us, length us, event | category | flops | bytes accessed | tf_op | source)
XLA Modules:
  0.0 115.8 jit_solution(10353204615117482983)
XLA Ops:
  0.0 115.0 %shard_map.73 = bf16[256,1024]{1,0:T(8,128)(2,1)S(1)} custom-call(bf16[256,1024]{1,0:T(8,128)(2,1)} %x_hbm.1, f32[1,1024]{1,0:T(1,128)} %bitcast.4, f32[1,1024]{1,0:T(1,128)} %bitcast.5, f32[1,1024]{1,0:T(1,128)} %bitcast.6, f32[1,1024]{1,0:T(1,128)} %bitcast.7, bf16[1024,8192]{1,0:T(8,128)(2,1)} %up_hbm.1, bf16[8192,1024]{1,0:T(8,128)(2,1)} %down_hbm.1), custom_call_target="tpu_custom_call" | custom-call | tf_op jit(solution)/shard_map/pallas_call | solution.py:408
  115.0 0.8 copy.9

commit v3 on v2

--- a/solution.py
+++ b/solution.py
@@ -12,21 +12,23 @@
 STAT_ROWS = 8
 EXTRA = 16
 ROWS = 128
+PARTS = 1
 CHUNK = 256
 RAW = 3
 LAG = 2
-AHEAD = 8
+AHEAD = 4
 LAG_STEP = 7
+KEEP = 4
 TOTAL_AT = 5
 LIMIT = 56
 
 
 def kernel(
-    n, n_ra, x_hbm, gain_in_hbm, shift_in_hbm, gain_out_hbm, shift_out_hbm, up_hbm, down_hbm, out_ref,
+    n, n_ra, parts, x_hbm, gain_in_hbm, shift_in_hbm, gain_out_hbm, shift_out_hbm, up_hbm, down_hbm, out_ref,
     x_v, vectors, up_v, down_v, tile_v, raw, raw_out, raw_in, sums, from_outer, from_partner, normed, mine,
     acc, acc_in, stats_in, stats_out,
     x_sem, vector_sem, up_sem, down_sem, raw_sent, raw_got, sums_sent, outer_got, partner_got,
-    hidden_sent, hidden_got, stat_sent, stat_got, acc_sent, acc_got,
+    hidden_sent, hidden_got, tail_sent, tail_got, stat_sent, stat_got, acc_sent, acc_got,
 ):
     me = lax.axis_index("cb")
     ra = lax.axis_index("ra")
@@ -34,6 +36,7 @@
     tokens = normed.shape[0]
     steps, rows = sums.shape[0], sums.shape[1]
     blocks = tokens // rows
+    part_rows = rows // parts
     half = n // 2
     ahead = min(AHEAD, chunks)
     n_raw = raw_out.shape[0]
@@ -50,6 +53,9 @@
     def block_of(b):
         return pl.ds(pl.multiple_of(b * rows, rows), rows)
 
+    def part_of(q):
+        return pl.ds(pl.multiple_of(q * part_rows, part_rows), part_rows)
+
     def x_copy(b):
         return pltpu.make_async_copy(x_hbm.at[block_of(b)], x_v.at[block_of(b)], x_sem.at[b])
 
@@ -86,25 +92,34 @@
         centred = values - total * (1.0 / depth)
         squares = jnp.sum(centred * centred, axis=1, keepdims=True)
         lane = lax.broadcasted_iota(jnp.int32, (values.shape[0], LANES), 1)
-        tile_v[pl.ds(0, rows)] = jnp.where(lane == 0, total, jnp.where(lane == 1, squares, 0.0))
+        tile_v[pl.ds(0, values.shape[0])] = jnp.where(lane == 0, total, jnp.where(lane == 1, squares, 0.0))
         return tile_v[...].T[:STAT_ROWS], centred
 
-    def stat_copy(stats, which, b, k, slot):
+    def stat_copy(stats, which, b, k, slot, core):
         return pltpu.make_async_remote_copy(
             src_ref=stats.at[b, slot], dst_ref=stats.at[b, slot],
-            send_sem=stat_sent.at[which, b, k], recv_sem=stat_got.at[which, b, slot],
-            device_id={"cb": lax.rem(me + k, n)}, device_id_type=MESH,
+            send_sem=stat_sent.at[which, b, core * n + k], recv_sem=stat_got.at[which, b, slot],
+            device_id={"cb": lax.rem(me + k, n), "ra": core}, device_id_type=MESH,
         )
 
+    def for_stats(stats, which, b, act):
+        if which == 0:
+            for k in range(1, n):
+                act(stat_copy(stats, which, b, k, me, ra))
+        else:
+            @pl.when(ra == n_ra - 1)
+            def _():
+                for k in range(1, n):
+                    for core in range(n_ra):
+                        act(stat_copy(stats, which, b, k, me, core))
+
     def send_stats(stats, which, b):
-        for k in range(1, n):
-            stat_copy(stats, which, b, k, me).start()
+        for_stats(stats, which, b, lambda copy: copy.start())
 
     def merged_stats(stats, which, b):
         for k in range(1, n):
-            stat_copy(stats, which, b, k, lax.rem(me + k, n)).wait_recv()
-        for k in range(1, n):
-            stat_copy(stats, which, b, k, me).wait_send()
+            stat_copy(stats, which, b, k, lax.rem(me + k, n), ra).wait_recv()
+        for_stats(stats, which, b, lambda copy: copy.wait_send())
         total = stats[b, 0][0:1]
         for j in range(1, n):
             total = total + stats[b, j][0:1]
@@ -118,10 +133,10 @@
         shift = stats[b, outer][0:1] * (1.0 / depth) - mean
         row = lax.broadcasted_iota(jnp.int32, (LANES, LANES), 0)
         tile = jnp.where(row == 0, mean, jnp.where(row == 1, scale, jnp.where(row == 2, shift, 0.0)))
-        return tile.T[:rows]
+        return tile.T
 
     def make_normed(b):
-        tile = merged_stats(stats_in, 0, b)
+        tile = merged_stats(stats_in, 0, b)[:rows]
         values = x_v[block_of(b)].astype(jnp.float32)
         normed[block_of(b)] = (
             (values - tile[:, 0:1]) * tile[:, 1:2] * vectors[0] + vectors[1]
@@ -146,10 +161,17 @@
             recv_sem=hidden_got.at[s], device_id={"cb": outer}, device_id_type=MESH,
         )
 
-    def acc_copy(k, b):
+    def tail_copy(h):
+        piece = hidden.at[steps - 1, pl.ds(h * part_rows, part_rows)]
         return pltpu.make_async_remote_copy(
-            src_ref=acc.at[block_of(b)], dst_ref=acc_in.at[k - 1, block_of(b)],
-            send_sem=acc_sent.at[k - 1, b], recv_sem=acc_got.at[k - 1, b],
+            src_ref=piece, dst_ref=piece, send_sem=tail_sent.at[h], recv_sem=tail_got.at[h],
+            device_id={"cb": outer}, device_id_type=MESH,
+        )
+
+    def acc_copy(k, q):
+        return pltpu.make_async_remote_copy(
+            src_ref=acc.at[part_of(q)], dst_ref=acc_in.at[k - 1, part_of(q)],
+            send_sem=acc_sent.at[k - 1, q], recv_sem=acc_got.at[k - 1, q],
             device_id={"ra": lax.rem(ra + k, n_ra)}, device_id_type=MESH,
         )
 
@@ -205,6 +227,9 @@
         tile_v[...] = jnp.zeros_like(tile_v)
 
     def first_pass(s, weight):
+        if isinstance(s, int) and s >= chunks:
+            return
+
         @pl.when(s < chunks)
         def _():
             weight(s)
@@ -229,12 +254,32 @@
 
         @pl.when(c == chunks - 1)
         def _():
+            for h in range(parts):
+                for k in range(1, n_ra):
+                    acc_copy(k, b * parts + h).start()
+
+        @pl.when((b > 0) & (c == min(TOTAL_AT, chunks - 1)))
+        def _():
+            for h in range(parts):
+                make_total((b - 1) * parts + h)
+
+        @pl.when((b > 0) & (c == chunks - 2))
+        def _():
+            for h in range(parts):
+                make_out((b - 1) * parts + h)
+
+    def finish_down(wait):
+        first_pass(steps - 1, want_down)
+        for h in range(parts):
+            if wait:
+                tail_copy(h).wait_recv()
+            q = (blocks - 1) * parts + h
+            acc[part_of(q)] += jnp.dot(
+                hidden[steps - 1, pl.ds(h * part_rows, part_rows)], down_v[chunks - 1],
+                preferred_element_type=jnp.float32,
+            )
             for k in range(1, n_ra):
-                acc_copy(k, b).start()
-
-        @pl.when((b > 0) & (c == TOTAL_AT))
-        def _():
-            make_total(b - 1)
+                acc_copy(k, q).start()
 
     def take_outer(s):
         sum_copy(s, from_outer, outer_got).wait_recv()
@@ -252,6 +297,19 @@
             sum_copy(s, from_partner, partner_got).start()
         else:
             sum_copy(s, from_outer, outer_got).start()
+
+    def take_last(mid):
+        if mid:
+            sum_copy(steps - 1, from_partner, partner_got).wait_recv()
+        for h in range(parts):
+            piece = pl.ds(h * part_rows, part_rows)
+            if mid:
+                full = sums[steps - 1, piece].astype(jnp.float32) + from_partner[steps - 1, piece].astype(jnp.float32)
+                hidden[steps - 1, piece] = jnp.square(jnp.maximum(full, 0.0)).astype(jnp.bfloat16)
+            else:
+                tail_copy(h).wait_recv()
+            if half > 1:
+                tail_copy(h).start()
 
     def take_hidden(s, mid):
         if mid:
@@ -305,6 +363,11 @@
             add_down(s - lag - 1)
             next_up(s + 1)
             take_hidden(s - lag, mid)
+            sum_copy(s - lag - 1, from_outer, outer_got).wait_send()
+            if half > 1:
+                @pl.when(s > lag + KEEP)
+                def _():
+                    hidden_copy(s - lag - 1 - KEEP).wait_send()
             after_up(s + 1)
             after_down(s - lag - 1)
 
@@ -314,16 +377,18 @@
             sums[steps - 1] = mine[(steps - 1) % 2].astype(jnp.bfloat16)
         give(steps - 1, mid)
 
-        @pl.loop(steps - 1, steps + lag)
+        @pl.loop(steps - 1, steps + lag - 1)
         def _(s):
             first_pass(s - lag - 1, want_down)
             add_down(s - lag - 1)
             after_down(s - lag - 1)
             take_hidden(s - lag, mid)
 
-        first_pass(steps - 1, want_down)
-        add_down(steps - 1)
-        after_down(steps - 1)
+        first_pass(steps - 2, want_down)
+        add_down(steps - 2)
+        after_down(steps - 2)
+        take_last(mid)
+        finish_down(False)
 
     def source():
         @pl.loop(n_raw, steps)
@@ -333,29 +398,39 @@
             sum_copy(s, from_outer, outer_got).start()
             after_up(s)
 
-        @pl.loop(0, steps)
+        @pl.loop(0, steps - 1)
         def _(s):
             hidden_copy(s).wait_recv()
             first_pass(s, want_down)
             add_down(s)
+
+            @pl.when(s < n_raw)
+            def _():
+                raw_copy(s).wait_send()
+
+            @pl.when(s >= n_raw)
+            def _():
+                sum_copy(s, from_outer, outer_got).wait_send()
             after_down(s)
 
-    def make_total(b):
-        block = block_of(b)
+        finish_down(True)
+
+    def make_total(q):
+        block = part_of(q)
         for k in range(1, n_ra):
-            acc_copy(k, b).wait()
+            acc_copy(k, q).wait()
         branch = acc[block]
         for k in range(1, n_ra):
             branch = branch + acc_in[k - 1, block]
         total = 2.0**0.25 * normed[block].astype(jnp.float32) + branch
         acc[block] = total
-        stats_out[b, me] = row_stats(total)[0]
-        send_stats(stats_out, 1, b)
-
-    def make_out(b):
-        tile = merged_stats(stats_out, 1, b)
-        out_ref[block_of(b)] = (
-            (acc[block_of(b)] - tile[:, 0:1]) * tile[:, 1:2] * vectors[2] + vectors[3]
+        stats_out[q, me] = row_stats(total)[0]
+        send_stats(stats_out, 1, q)
+
+    def make_out(q):
+        tile = merged_stats(stats_out, 1, q)[:part_rows]
+        out_ref[part_of(q)] = (
+            (acc[part_of(q)] - tile[:, 0:1]) * tile[:, 1:2] * vectors[2] + vectors[3]
         ).astype(jnp.bfloat16)
 
     vector_copy(2).wait()
@@ -366,27 +441,26 @@
     if half > 2:
         pl.when((level > 0) & (level < half - 1))(functools.partial(relay, False))
 
-    make_total(blocks - 1)
-
-    @pl.when(sends_raw)
-    def _():
-        @pl.loop(0, n_raw)
-        def _(c):
-            raw_copy(c).wait_send()
-
-    @pl.loop(jnp.where(sends_raw, n_raw, 0), steps)
+    for h in range(parts):
+        make_total((blocks - 1) * parts + h)
+
+    lag = LAG + jnp.where(is_mid, 0, LAG_STEP * (half - 1 - level))
+
+    @pl.loop(jnp.where(sends_raw, steps - 1, steps - lag - 2), steps)
     def _(s):
         sum_copy(s, from_outer, outer_got).wait_send()
 
     @pl.when(has_outer)
     def _():
-        @pl.loop(0, steps)
+        @pl.loop(steps - lag - 2 - KEEP, steps - 1)
         def _(s):
             hidden_copy(s).wait_send()
 
-    @pl.loop(0, blocks)
-    def _(b):
-        make_out(b)
+        for h in range(parts):
+            tail_copy(h).wait_send()
+
+    for h in range(parts):
+        make_out((blocks - 1) * parts + h)
 
 
 def solution(mesh):
@@ -399,6 +473,7 @@
         chunks = units // width
         rows = ROWS if tokens % ROWS == 0 else tokens
         blocks = tokens // rows
+        parts = PARTS if rows % (PARTS * 16) == 0 else 1
         n_raw = min(RAW, LAG + 1, chunks)
         vmem = pl.BlockSpec(memory_space=pltpu.VMEM)
         hbm = pl.BlockSpec(memory_space=pl.ANY)
@@ -406,7 +481,7 @@
         vectors = [vector.reshape(1, depth) for vector in (gain_in, shift_in, gain_out, shift_out)]
         operands = [residual_in, *vectors, up_weight, down_weight]
         return pl.pallas_call(
-            functools.partial(kernel, n, n_ra),
+            functools.partial(kernel, n, n_ra, parts),
             out_shape=pltpu.VMEM((tokens, depth), jnp.bfloat16),
             in_specs=[hbm] * 7,
             out_specs=vmem,
@@ -427,15 +502,16 @@
                 pltpu.VMEM((tokens, depth), jnp.float32),
                 pltpu.VMEM((n_ra - 1, tokens, depth), jnp.float32),
                 pltpu.VMEM((blocks, n, STAT_ROWS, LANES), jnp.float32),
-                pltpu.VMEM((blocks, n, STAT_ROWS, LANES), jnp.float32),
+                pltpu.VMEM((blocks * parts, n, STAT_ROWS, LANES), jnp.float32),
                 pltpu.SemaphoreType.DMA((blocks,)),
                 pltpu.SemaphoreType.DMA((4,)),
             ]
             + [pltpu.SemaphoreType.DMA((chunks,))] * 2
             + [pltpu.SemaphoreType.DMA((n_raw,))] * 2
             + [pltpu.SemaphoreType.DMA((chunks * blocks,))] * 5
-            + [pltpu.SemaphoreType.DMA((2, blocks, n))] * 2
-            + [pltpu.SemaphoreType.DMA((n_ra - 1, blocks))] * 2,
+            + [pltpu.SemaphoreType.DMA((parts,))] * 2
+            + [pltpu.SemaphoreType.DMA((2, blocks * parts, n_ra * n)), pltpu.SemaphoreType.DMA((2, blocks * parts, n))]
+            + [pltpu.SemaphoreType.DMA((n_ra - 1, blocks * parts))] * 2,
             compiler_params=pltpu.CompilerParams(
                 collective_id=0, has_side_effects=True, vmem_limit_bytes=LIMIT * 1024 * 1024
             ),

time: 116 us -> 116 us (level)
  no operation moved by 1% of the time
where the time goes in v3:
time: 116 us; the launch traced here: 115 us
  Pallas kernels  115 us (99%)
    pallas_call x1, Pallas kernels, per_device(): pl.pallas_call(functools.partial(kernel, n, n_ra, parts), out_shape=pltpu...  115 us

profile of v3, /device:TPU:0, one launch (start us, length us, event | category | flops | bytes accessed | tf_op | source)
XLA Modules:
  0.0 115.4 jit_solution(17849101799238970786)
XLA Ops:
  0.0 114.6 %shard_map.73 = bf16[256,1024]{1,0:T(8,128)(2,1)S(1)} custom-call(bf16[256,1024]{1,0:T(8,128)(2,1)} %x_hbm.1, f32[1,1024]{1,0:T(1,128)} %bitcast.4, f32[1,1024]{1,0:T(1,128)} %bitcast.5, f32[1,1024]{1,0:T(1,128)} %bitcast.6, f32[1,1024]{1,0:T(1,128)} %bitcast.7, bf16[1024,8192]{1,0:T(8,128)(2,1)} %up_hbm.1, bf16[8192,1024]{1,0:T(8,128)(2,1)} %down_hbm.1), custom_call_target="tpu_custom_call" | custom-call | tf_op jit(solution)/shard_map/pallas_call | solution.py:483
  114.6 0.8 copy.9

commit v4 on v3

--- a/solution.py
+++ b/solution.py
@@ -200,15 +200,24 @@
             row == 0, vectors[0], jnp.where(row == 1, vectors[1], 0.0)
         ).astype(jnp.bfloat16)
 
+    def raw_part(c):
+        want_up(c)
+        raw_out[c] = jnp.dot(raw[...], up_v[c], preferred_element_type=jnp.float32).astype(jnp.bfloat16)
+
+    @pl.when(sends_raw)
+    def _():
+        raw_part(0)
+
     pl.semaphore_wait(barrier, n - 1 + n_ra - 1)
     send_stats(stats_in, 0, 0)
 
     @pl.when(sends_raw)
     def _():
-        @pl.loop(0, n_raw)
+        raw_copy(0).start()
+
+        @pl.loop(1, n_raw)
         def _(c):
-            want_up(c)
-            raw_out[c] = jnp.dot(raw[...], up_v[c], preferred_element_type=jnp.float32).astype(jnp.bfloat16)
+            raw_part(c)
             raw_copy(c).start()
 
     @pl.loop(1, blocks)

time: 116 us -> 116 us (level)
  no operation moved by 1% of the time
where the time goes in v4:
time: 116 us; the launch traced here: 115 us
  Pallas kernels  115 us (99%)
    pallas_call x1, Pallas kernels, per_device(): pl.pallas_call(functools.partial(kernel, n, n_ra, parts), out_shape=pltpu...  115 us

profile of v4, /device:TPU:0, one launch (start us, length us, event | category | flops | bytes accessed | tf_op | source)
XLA Modules:
  0.0 115.4 jit_solution(10265767076470774839)
XLA Ops:
  0.0 114.5 %shard_map.73 = bf16[256,1024]{1,0:T(8,128)(2,1)S(1)} custom-call(bf16[256,1024]{1,0:T(8,128)(2,1)} %x_hbm.1, f32[1,1024]{1,0:T(1,128)} %bitcast.4, f32[1,1024]{1,0:T(1,128)} %bitcast.5, f32[1,1024]{1,0:T(1,128)} %bitcast.6, f32[1,1024]{1,0:T(1,128)} %bitcast.7, bf16[1024,8192]{1,0:T(8,128)(2,1)} %up_hbm.1, bf16[8192,1024]{1,0:T(8,128)(2,1)} %down_hbm.1), custom_call_target="tpu_custom_call" | custom-call | tf_op jit(solution)/shard_map/pallas_call | solution.py:492
  114.6 0.8 copy.9
